TPU v7x, 32 devices: a whole 2x2x4 slice. The times are simulated.
32 devices in a mesh: sp: 16 (over z, y, x), tp: 2 (over core).
Axes of the slice: x: 2, y: 2, z: 4, core: 2. Of those that a mesh axis runs over, the one named last changes fastest.
Arguments:
- queries: bfloat16 [3, 4096, 2048], P(None, 'sp', 'tp'), may hold values from -6 to 6
- keys: bfloat16 [3, 4096, 2048], P(None, 'sp', 'tp'), may hold values from -6 to 6
- values: bfloat16 [3, 4096, 2048], P(None, 'sp', 'tp'), may hold values from -6 to 6
- w_out: bfloat16 [2048, 2048], P(None, 'tp'), may hold values from -1 to 1
Outputs:
- mixed: bfloat16 [4096, 2048], P('sp', 'tp')
All inputs are finite; a program needn't handle non-finite values.
Results may differ from a plain program's by a relative error of at most 0.01.
Values may be sent and summed in bfloat16 or wider, within the bound.
A program may use at most 128 MiB of HBM per device.

v0:
```python
import jax
import jax.numpy as jnp
from jax import lax
from jax.sharding import PartitionSpec as P

HEAD = 128
KEYS_PER_QUERY = 128
FIRST_STRIDE = 1
SECOND_STRIDE = 4
THIRD_STRIDE = 16


ROPE_BASE = 10000.0
MASKED = -1e30


def shifted(block, axis, distance):
    devices = range(lax.axis_size(axis))
    route = [(i - distance, i) for i in devices if i - distance in devices]
    return lax.ppermute(block, axis, route)


def turn_halves(matrix, cosine, sine_part):
    first_half, second_half = jnp.split(matrix, 2, axis=-1)
    return jnp.concatenate(
        [
            first_half * cosine - second_half * sine_part,
            second_half * cosine + first_half * sine_part,
        ],
        axis=-1,
    )


def local_window(query_in, extended, dilation, start_pos):
    row_count = query_in.shape[0]
    head_count = query_in.shape[1] // HEAD
    back_rows = KEYS_PER_QUERY * dilation
    strided = row_count // dilation
    block_len = min(strided, KEYS_PER_QUERY)
    block_count = strided // block_len
    q_blocks = query_in.reshape(block_count, block_len, dilation, head_count, HEAD)
    key_all = extended[0].reshape(strided + KEYS_PER_QUERY, dilation, head_count, HEAD)
    value_all = extended[1].reshape(strided + KEYS_PER_QUERY, dilation, head_count, HEAD)
    key_blocks = jnp.stack(
        [
            key_all[member * block_len : member * block_len + block_len + KEYS_PER_QUERY]
            for member in range(block_count)
        ]
    )
    value_blocks = jnp.stack(
        [
            value_all[member * block_len : member * block_len + block_len + KEYS_PER_QUERY]
            for member in range(block_count)
        ]
    )
    scores = jnp.einsum(
        "nqrhe,nkrhe->nrhqk", q_blocks, key_blocks, preferred_element_type=jnp.float32
    )
    grid_shape = (block_count, dilation, 1, block_len, block_len + KEYS_PER_QUERY)
    b_index = lax.broadcasted_iota(jnp.int32, grid_shape, 0)
    r_index = lax.broadcasted_iota(jnp.int32, grid_shape, 1)
    q_index = lax.broadcasted_iota(jnp.int32, grid_shape, 3)
    k_index = lax.broadcasted_iota(jnp.int32, grid_shape, 4)
    distance = q_index + KEYS_PER_QUERY - k_index
    position = start_pos - back_rows + (b_index * block_len + k_index) * dilation + r_index
    allowed = (distance >= 0) & (distance <= KEYS_PER_QUERY) & (position >= 0)
    scores = jnp.where(allowed, scores, MASKED)
    row_max = jnp.max(scores, axis=-1, keepdims=True)
    weights = jnp.exp(scores - row_max)
    row_sum = jnp.sum(weights, axis=-1, keepdims=True)
    weighted = jnp.einsum(
        "nrhqk,nkrhe->nqrhe",
        weights.astype(jnp.bfloat16),
        value_blocks,
        preferred_element_type=jnp.float32,
    )
    divisor = jnp.transpose(row_sum[..., 0], (0, 3, 1, 2))[..., None]
    result = (weighted / divisor).reshape(row_count, head_count, HEAD)
    log_sum = jnp.transpose((row_max + jnp.log(row_sum))[..., 0], (0, 3, 1, 2)).reshape(
        row_count, head_count
    )
    return (result, log_sum)


def shards(queries, keys, values, w_out):
    token_count = queries.shape[1]
    features = queries.shape[2]
    head_count = features // HEAD
    start_pos = lax.axis_index("sp") * token_count
    positions = (lax.iota(jnp.int32, token_count) + start_pos).astype(jnp.float32)
    inverse = ROPE_BASE ** (-jnp.arange(0, HEAD, 2, dtype=jnp.float32) / HEAD)
    angles = positions[:, None] * inverse[None, :]
    cosine = jnp.cos(angles)[:, None, :]
    sine_part = jnp.sin(angles)[:, None, :]
    group_strides = (FIRST_STRIDE, SECOND_STRIDE, THIRD_STRIDE)
    turned = []
    stacked = []
    for group_id in range(len(group_strides)):
        query_f = queries[group_id].astype(jnp.float32).reshape(token_count, head_count, HEAD)
        key_f = keys[group_id].astype(jnp.float32).reshape(token_count, head_count, HEAD)
        turned_q = (turn_halves(query_f, cosine, sine_part) * HEAD ** (-0.5)).astype(jnp.bfloat16)
        turned_k = turn_halves(key_f, cosine, sine_part).astype(jnp.bfloat16)
        turned.append(turned_q.reshape(token_count, features))
        stacked.append(jnp.stack([turned_k.reshape(token_count, features), values[group_id]]))
    closest_rows = KEYS_PER_QUERY * FIRST_STRIDE
    near_prev = shifted(stacked[0][:, token_count - closest_rows :, :], "sp", 1)
    extended = [jnp.concatenate([near_prev, stacked[0]], axis=1)]
    group_spans = [
        -(-(KEYS_PER_QUERY * key_stride) // token_count) for key_stride in group_strides[1:]
    ]

    def trimmed(fragment, member, arrival):
        if arrival == group_spans[member]:
            return fragment
        return fragment

    def unpack(arrived, members, sizes, pieces):
        cursor = 0
        for member, count in zip(members, sizes):
            pieces[member].append(arrived[:, cursor : cursor + count, :])
            cursor += count

    pieces = [[stacked[1]], [stacked[2]]]
    covered = 1
    while covered < max(group_spans) + 1:
        amounts = [max(0, min(covered, group_spans[member] + 1 - covered)) for member in range(2)]
        members = []
        fragments = []
        for member in range(2):
            for step_index in range(amounts[member]):
                members.append(member)
                fragments.append(trimmed(pieces[member][step_index], member, covered + step_index))
        payload = jnp.concatenate(fragments, axis=1)
        arrived = shifted(payload, "sp", covered)
        unpack(arrived, members, [fragment.shape[1] for fragment in fragments], pieces)
        covered *= 2
    for member in range(2):
        ordered = [
            pieces[member][group_spans[member] - offset] for offset in range(group_spans[member])
        ]
        joined = jnp.concatenate(ordered + [pieces[member][0]], axis=1)
        extended.append(joined)
    results = []
    log_sums = []
    for group_id in range(len(group_strides)):
        result, log_sum = local_window(
            turned[group_id], extended[group_id], group_strides[group_id], start_pos
        )
        results.append(result)
        log_sums.append(log_sum)
    shares = jax.nn.softmax(jnp.stack(log_sums), axis=0)
    attended = jnp.sum(shares[..., None] * jnp.stack(results), axis=0)
    attended = attended.astype(jnp.bfloat16).reshape(token_count, features)
    mixed_out = jnp.dot(
        lax.all_gather(attended, "tp", axis=1, tiled=True),
        w_out,
        preferred_element_type=jnp.float32,
    )
    return mixed_out.astype(jnp.bfloat16)


def solution(mesh):
    return jax.shard_map(
        shards,
        mesh=mesh,
        in_specs=(P(None, "sp", "tp"), P(None, "sp", "tp"), P(None, "sp", "tp"), P(None, "tp")),
        out_specs=P("sp", "tp"),
        check_vma=False,
    )
```

profile of v0, /device:TPU:21, one launch (start us, length us, event | category | flops | bytes accessed | tf_op | source)
XLA Modules:
  0.0 429.9 jit_solution(7861315412004716294)
XLA Ops:
  6.6 1.5 fusion.98
  11.9 2.4 copy.126
  15.2 2.5 copy.119
  24.7 2.3 copy.133
  27.9 2.4 copy.129
  31.2 2.4 copy.122
  38.1 7.1 %multiply_subtract_fusion.2 = (f32[256,8,64]{2,0,1:T(8,128)}, f32[256,8,64]{2,0,1:T(8,128)}, bf16[256,8,64]{2,0,1:T(8,128)(2,1)S(1)}, bf16[256,8,64]{2,0,1:T(8,1...) fusion(f32[256,8,64]{2,0,1:T(8,128)} %copy.119, ...), kind=kLoop, calls=%fused_computation.70 | loop fusion | flops 5505024 | bytes 11141120 | tf_op jit(solution)/shard_map/sub | solution.py:27
  45.7 2.5 pad_maximum_fusion.8
  48.5 2.3 fusion.100
  51.3 3.1 collective-permute-start.1
  54.4 46.2 %collective-permute-done.1 = bf16[2,512,1024]{1,2,0:T(8,128)(2,1)S(1)} collective-permute-done((bf16[2,512,1024]{1,2,0:T(8,128)(2,1)S(1)}, bf16[2,512,1024]{1,2,0:T(8,128)(2,1)S(1)}, u32[]{:S(2)}, u32[]{:S(2)}) %collective-permute-start.1) | collective-permute-done | bytes 2097184 | tf_op jit(solution)/shard_map/ppermute | solution.py:20
  102.3 4.0 collective-permute-start.2
  106.4 66.0 %collective-permute-done.2 = bf16[2,768,1024]{1,2,0:T(8,128)(2,1)S(1)} collective-permute-done((bf16[2,768,1024]{1,2,0:T(8,128)(2,1)S(1)}, bf16[2,768,1024]{1,2,0:T(8,128)(2,1)S(1)}, u32[]{:S(2)}, u32[]{:S(2)}) %collective-permute-start.2) | collective-permute-done | bytes 3145760 | tf_op jit(solution)/shard_map/ppermute | solution.py:20
  172.3 1.6 copy-done
  174.1 2.3 pad_maximum_fusion
  176.4 3.2 collective-permute-start.4
  181.9 2.2 collective-permute-start
  186.7 2.5 copy.80
  189.2 2.4 copy.79
  195.8 2.1 pad_maximum_fusion.6
  199.3 2.1 copy.107
  201.3 2.9 select_reduce_fusion.2
  206.0 1.7 copy.109
  207.6 83.1 %collective-permute-done.3 = bf16[2,256,1024]{1,2,0:T(8,128)(2,1)} collective-permute-done((bf16[2,256,1024]{1,2,0:T(8,128)(2,1)}, bf16[2,256,1024]{1,2,0:T(8,128)(2,1)}, u32[]{:S(2)}, u32[]{:S(2)}) %collective-permute-start.3) | collective-permute-done | bytes 1048608 | tf_op jit(solution)/shard_map/ppermute | solution.py:20
  290.8 2.4 constant_dynamic-update-slice_fusion.2
  293.1 2.4 slice_dynamic-update-slice_fusion.5
  295.5 2.5 slice_dynamic-update-slice_fusion.4
  298.1 2.3 slice_dynamic-update-slice_fusion.3
  300.4 2.3 slice_dynamic-update-slice_fusion.2
  303.9 1.5 fusion.96
  305.4 1.6 fusion.97
  308.1 8.1 %fusion.94 = (bf16[1,2304,1024]{1,2,0:T(8,128)(2,1)}, bf16[1,2304,1024]{1,2,0:T(8,128)(2,1)}) fusion(bf16[2,2304,1024]{1,2,0:T(8,128)(2,1)} %constant_dynamic-update-slice_fusion), kind=kLoop, calls=%fused_computation.144 | loop fusion | bytes 18874368 | tf_op jit(solution)/shard_map/slice | solution.py:42
  316.1 6.7 %copy.99 = bf16[1,2304,1024]{2,1,0:T(8,128)(2,1)} copy(bf16[1,2304,1024]{1,2,0:T(8,128)(2,1)} %get-tuple-element.5) | data formatting | bytes 9437184 | tf_op jit(solution)/shard_map/slice | solution.py:42
  322.8 3.7 copy.139
  326.5 5.1 %select_reduce_fusion = (f32[16,8,16]{2,1,0:T(8,128)S(1)}, f32[16,8,16,144]{3,2,1,0:T(8,128)S(1)}) fusion(pred[16,16,144]{2,1,0:T(8,128)(4,1)S(1)} %fusion.73, bf16[144,16,8,128]{3,2,1,0:T(8,128)(2,1)S(1)} %bitcast.146, f32[16,16,8,64]{3,0,2,1:T(8,128)S(1)} %copy-done.8, f32[16,16,8,64]{3,0,2,1:T(8,128)S(1)} %copy-done.9), kind=kOutput, calls=%fused_computation.13 | convolution fusion | flops 76871680 | bytes 6991872 | tf_op jit(solution)/shard_map/nqrhe,nkrhe->nrhqk/dot_general | solution.py:56
  333.5 1.7 maximum_maximum_fusion
  335.2 1.8 fusion.95
  337.0 2.7 copy.91
  339.7 1.9 copy.138
  345.6 2.6 copy.110
  348.2 2.0 copy.140
  350.2 1.9 fusion.51
  354.3 6.7 %copy.113 = bf16[1,2304,1024]{2,1,0:T(8,128)(2,1)} copy(bf16[1,2304,1024]{1,2,0:T(8,128)(2,1)} %get-tuple-element.6) | data formatting | bytes 9437184 | tf_op jit(solution)/shard_map/slice | solution.py:43
  361.0 3.6 copy.141
  364.6 4.7 %fusion.46 = f32[1,16,16,8,128]{4,1,3,2,0:T(8,128)S(1)} fusion(bf16[144,16,8,128]{3,2,1,0:T(8,128)(2,1)S(1)} %bitcast.165, f32[16,8,16,144]{3,2,1,0:T(8,128)S(1)} %get-tuple-element.61, f32[16,8,16]{2,1,0:T(8,128)S(1)} %copy-done.17, pred[16,16,144]{2,1,0:T(8,128)(4,1)S(1)} %copy-done.19, f32[16,16,8]{0,2,1:T(8,128)S(1)} %bitcast.188), kind=kOutput, calls=%fused_computation.75 | convolution fusion | flops 76644352 | bytes 7000064 | tf_op jit(solution)/shard_map/nrhqk,nkrhe->nqrhe/dot_general | solution.py:71
  369.6 1.6 fusion.4
  372.2 46.3 %all-gather.2.cloned.1.call-done = bf16[256,2048]{1,0:T(8,128)(2,1)} async-done(((bf16[256,1024]{1,0:T(8,128)(2,1)}), bf16[256,2048]{1,0:T(8,128)(2,1)}) %all-gather.2.cloned.1.call-update) | async-done | bytes 1048592 | tf_op jit(solution)/shard_map/all_gather | solution.py:155
  418.5 4.6 %convolution_convert_fusion = bf16[256,1024]{1,0:T(8,128)(2,1)} fusion(bf16[256,2048]{1,0:T(8,128)(2,1)} %all-gather.2.cloned.1.call-done, bf16[2048,1024]{1,0:T(8,128)(2,1)} %param.7), kind=kOutput, calls=%fused_computation.29 | convolution fusion | flops 1074003968 | bytes 5767168 | tf_op jit(solution)/shard_map/dot_general | solution.py:154
  (124 shorter events, 44.6 us)
Async XLA Ops:
  6.5 411.9 %all-gather.2.cloned.1.call-start = ((), (), s32[]{:S(2)}) async-start(), calls=%async_computation | async-start | bytes 1572864 | tf_op jit(solution)/shard_map/all_gather | solution.py:155
  45.2 3.2 copy-start.4
  45.2 3.2 copy-start.5
  51.3 49.3 %collective-permute-start.1 = (bf16[2,512,1024]{1,2,0:T(8,128)(2,1)S(1)}, bf16[2,512,1024]{1,2,0:T(8,128)(2,1)S(1)}, u32[]{:S(2)}, u32[]{:S(2)}) collective-permute-start(bf16[2,512,1024]{1,2,0:T(8,128)(2,1)S(1)} %maximum_maximum_fusion.1), channel_id=1, source_target_pairs={{0,2},{2,4},{4,6},{6,8},{8,10},{10,12},{12,14},{14,16},{16,18},{18... | collective-permute-start | bytes 6291464 | tf_op jit(solution)/shard_map/ppermute | solution.py:20
  100.6 1.4 copy-start.6
  102.3 70.0 %collective-permute-start.2 = (bf16[2,768,1024]{1,2,0:T(8,128)(2,1)S(1)}, bf16[2,768,1024]{1,2,0:T(8,128)(2,1)S(1)}, u32[]{:S(2)}, u32[]{:S(2)}) collective-permute-start(bf16[2,768,1024]{1,2,0:T(8,128)(2,1)S(1)} %pad_maximum_fusion.1), channel_id=1, source_target_pairs={{0,4},{2,6},{4,8},{6,10},{8,12},{10,14},{12,16},{14,18},{16,20},{1... | collective-permute-start | bytes 9437192 | tf_op jit(solution)/shard_map/ppermute | solution.py:20
  172.3 1.6 copy-start
  174.1 5.5 %copy-start.15 = (bf16[256,8,128]{2,0,1:T(8,128)(2,1)S(1)}, bf16[256,8,128]{2,0,1:T(8,128)(2,1)}, u32[]{:S(2)}) copy-start(bf16[256,8,128]{2,0,1:T(8,128)(2,1)} %get-tuple-element.66) | copy-start | bytes 1572868
  176.4 116.7 %collective-permute-start.4 = (bf16[2,1024,1024]{1,2,0:T(8,128)(2,1)}, bf16[2,1024,1024]{1,2,0:T(8,128)(2,1)}, u32[]{:S(2)}, u32[]{:S(2)}) collective-permute-start(bf16[2,1024,1024]{1,2,0:T(8,128)(2,1)} %pad_maximum_fusion), channel_id=1, source_target_pairs={{0,8},{2,10},{4,12},{6,14},{8,16},{10,18},{12,20},{14,22},{16,24},... | collective-permute-start | bytes 12582920 | tf_op jit(solution)/shard_map/ppermute | solution.py:20
  181.9 13.9 %collective-permute-start = (bf16[2,128,1024]{1,2,0:T(8,128)(2,1)}, bf16[2,128,1024]{1,2,0:T(8,128)(2,1)}, u32[]{:S(2)}, u32[]{:S(2)}) collective-permute-start(bf16[2,128,1024]{1,2,0:T(8,128)(2,1)} %pad_maximum_fusion.7), channel_id=1, source_target_pairs={{0,2},{2,4},{4,6},{6,8},{8,10},{10,12},{12,14},{14,16},{16,18},{18... | collective-permute-start | bytes 1572872 | tf_op jit(solution)/shard_map/ppermute | solution.py:20
  185.3 105.5 %collective-permute-start.3 = (bf16[2,256,1024]{1,2,0:T(8,128)(2,1)}, bf16[2,256,1024]{1,2,0:T(8,128)(2,1)}, u32[]{:S(2)}, u32[]{:S(2)}) collective-permute-start(bf16[2,256,1024]{1,2,0:T(8,128)(2,1)} %pad_maximum_fusion.3), channel_id=1, source_target_pairs={{0,16},{2,18},{4,20},{6,22},{8,24},{10,26},{12,28},{14,30},{1,17},... | collective-permute-start | bytes 3145736 | tf_op jit(solution)/shard_map/ppermute | solution.py:20
  186.7 4.9 %copy-start.11 = (f32[256,8,64]{2,0,1:T(8,128)S(1)}, f32[256,8,64]{2,0,1:T(8,128)}, u32[]{:S(2)}) copy-start(f32[256,8,64]{2,0,1:T(8,128)} %get-tuple-element.56) | copy-start | bytes 1572868
  186.7 6.3 %copy-start.10 = (f32[256,8,64]{2,0,1:T(8,128)S(1)}, f32[256,8,64]{2,0,1:T(8,128)}, u32[]{:S(2)}) copy-start(f32[256,8,64]{2,0,1:T(8,128)} %get-tuple-element.57) | copy-start | bytes 1572868
  195.6 136.1 %copy-start.18 = (pred[16,16,144]{2,1,0:T(8,128)(4,1)}, pred[16,16,144]{2,1,0:T(8,128)(4,1)S(1)}, u32[]{:S(2)}) copy-start(pred[16,16,144]{2,1,0:T(8,128)(4,1)S(1)} %fusion.73) | copy-start | bytes 110596
  201.3 3.8 copy-start.20
  201.3 3.8 copy-start.21
  295.5 7.2 %copy-start.1 = (bf16[2,768,1024]{1,2,0:T(8,128)(2,1)S(1)}, bf16[2,768,1024]{1,2,0:T(8,128)(2,1)}, u32[]{:S(2)}) copy-start(bf16[2,768,1024]{1,2,0:T(8,128)(2,1)} %copy-done) | copy-start | bytes 9437188
  302.7 2.7 copy-start.7
  322.8 3.7 copy-start.8
  322.8 3.7 copy-start.9
  331.6 1.0 copy-start.16
  332.6 0.6 copy-start.22
  337.0 4.7 %copy-start.12 = (f32[64,4,8,64]{3,0,2,1:T(8,128)S(1)}, f32[64,4,8,64]{3,0,2,1:T(8,128)}, u32[]{:S(2)}) copy-start(f32[64,4,8,64]{3,0,2,1:T(8,128)} %copy.80) | copy-start | bytes 1572868
  339.7 2.0 copy-start.13
  343.1 1.4 copy-start.2
  348.2 2.1 copy-start.3
  361.0 3.6 copy-start.17
  361.0 3.6 copy-start.19
  361.0 3.6 copy-start.23
  364.6 5.0 %copy-start.14 = (f32[2,128,1,8,128]{4,3,1,0,2:T(8,128)S(1)}, f32[2,128,1,8,128]{4,3,1,0,2:T(8,128)}, u32[]{:S(2)}) copy-start(f32[2,128,1,8,128]{4,3,1,0,2:T(8,128)} %copy.109) | copy-start | bytes 3145732
Sparse Core Ops, SparseCore 0:
  372.3 46.0 all-gather.1
where the time goes:
time: 432 us; the launch traced here: 430 us
  waiting for transfers between devices  242 us (56%)
  local copies, waits for them, and re-layouts  114 us (26%)
  other arithmetic  25.3 us (6%)
  matrix products  21.3 us (5%)
  starting transfers between devices  14 us (3%)
  between operations  14 us (3%)
    ppermute x5, waiting for transfers between devices, shifted(): return lax.ppermute(block, axis, route)  195 us
    unnamed x80, local copies, waits for them, and re-layouts  54.5 us
    all_gather x1, waiting for transfers between devices, shards(): lax.all_gather(attended, 'tp', axis=1, tiled=True)  46.3 us
    slice x4, local copies, waits for them, and re-layouts, local_window(): extended[0].reshape(strided + KEYS_PER_QUERY, dilation, head_count, HEAD)  19.2 us
    ppermute x5, starting transfers between devices, shifted(): return lax.ppermute(block, axis, route)  14 us
    dot_general x3, matrix products, local_window(): jnp.einsum('nqrhe,nkrhe->nrhqk', q_blocks, key_blocks, preferred_element_...  9.41 us
    slice x2, local copies, waits for them, and re-layouts, local_window(): extended[1].reshape(strided + KEYS_PER_QUERY, dilation, head_count, HEAD)  9.29 us
  transfers between devices with their start and end apart: 6, of which 5 were waited for; matrix products, arithmetic and copies ran while one was open for 6% of the time, Pallas kernels for 0%

commit v1 on v0

v1 whole, which is shorter than its diff:
```python
import functools

import jax
import jax.numpy as jnp
from jax import lax
from jax.experimental import pallas as pl
from jax.experimental.pallas import tpu as pltpu
from jax.sharding import PartitionSpec as P

HEAD = 128
KEYS = 128
STRIDES = (1, 4, 16)
ROPE_BASE = 10000.0
MASKED = -1e30
TEAM = 4

MESH = pl.DeviceIdType.MESH
F32 = jnp.float32
BF16 = jnp.bfloat16


def kernel(
    cfg,
    q_in, k_in, v_in, w_in, cos_ref, sin_ref,
    o_ref,
    raw, ready, w_buf, tables, perms, q_buf, kv0, kv1, kv2, acc, top, den, att, full,
    in_sem, w_sem, deal_send, deal_recv, hop_send, hop_recv, ret_send, ret_recv, d2d_send, d2d_recv,
):
    tokens, n_sp, heads = cfg
    width = heads * HEAD
    mine = heads // TEAM
    part = mine * HEAD
    span = TEAM * tokens
    sp = lax.axis_index("sp")
    tp = lax.axis_index("tp")
    team = sp // TEAM
    me = lax.rem(sp, TEAM)
    has_next = sp + TEAM < n_sp
    has_prev = sp >= TEAM
    has_prev2 = sp >= 2 * TEAM

    inputs = (q_in, k_in, v_in)
    Q, K, V = 0, 1, 2
    order = [(V, 2), (K, 2), (V, 1), (K, 1), (V, 0), (K, 0), (Q, 1), (Q, 0), (Q, 2)]
    loads = {}
    for kind, g in order:
        copy = pltpu.make_async_copy(inputs[kind].at[g], raw.at[kind, g], in_sem.at[kind, g])
        copy.start()
        loads[kind, g] = copy
    w_copy = pltpu.make_async_copy(w_in, w_buf, w_sem)
    w_copy.start()

    barrier = pltpu.get_barrier_semaphore()
    for d in range(1, TEAM):
        peer = team * TEAM + lax.rem(me + d, TEAM)
        pl.semaphore_signal(barrier, inc=1, device_id={"sp": peer}, device_id_type=MESH)
    pl.semaphore_signal(barrier, inc=1, device_id={"tp": 1 - tp}, device_id_type=MESH)

    @pl.when(has_next)
    def _():
        pl.semaphore_signal(barrier, inc=1, device_id={"sp": sp + TEAM}, device_id_type=MESH)

    @pl.when(has_prev)
    def _():
        pl.semaphore_signal(barrier, inc=1, device_id={"sp": sp - TEAM}, device_id_type=MESH)

    row = lax.broadcasted_iota(jnp.int32, (tokens, tokens), 0)
    col = lax.broadcasted_iota(jnp.int32, (tokens, tokens), 1)
    for g in (1, 2):
        stride = STRIDES[g]
        each = tokens // stride
        origin = lax.rem(row, each) * stride + row // each
        perms[g - 1] = jnp.where(origin == col, 1.0, 0.0).astype(BF16)
    for g in range(3):
        stride = STRIDES[g]
        each = tokens // stride
        for r in range(stride):
            tables[0, g, r * each : (r + 1) * each, :] = cos_ref[pl.ds(r, each, stride=stride), :]
            tables[1, g, r * each : (r + 1) * each, :] = sin_ref[pl.ds(r, each, stride=stride), :]

    def prepare(kind, g):
        loads[kind, g].wait()

        def step(h, carry):
            lanes = pl.ds(pl.multiple_of(h * HEAD, HEAD), HEAD)
            x = raw[kind, g, :, lanes]
            if g > 0:
                x = jnp.dot(perms[g - 1], x, preferred_element_type=F32)
            else:
                x = x.astype(F32)
            if kind != V:
                x = x * tables[0, g] + pltpu.roll(x, HEAD // 2, 1) * tables[1, g]
            if kind == Q:
                x = x * HEAD ** (-0.5)
            ready[kind, g, :, lanes] = x.astype(BF16)
            return carry

        lax.fori_loop(0, heads, step, 0, unroll=2)

    def slot(kind, g, s):
        if kind == Q:
            return q_buf.at[g, s]
        if g == 2:
            return kv2.at[kind - 1, 2 * TEAM + s]
        if g == 1:
            return kv1.at[kind - 1, 2 + s]
        return kv0.at[kind - 1, pl.ds(pl.multiple_of(KEYS + s * tokens, KEYS), tokens)]

    def lanes_of(j):
        return pl.ds(pl.multiple_of(j * part, part), part)

    def deal(kind, g, d):
        peer = lax.rem(me + d, TEAM)
        return pltpu.make_async_remote_copy(
            src_ref=ready.at[kind, g, :, lanes_of(peer)],
            dst_ref=slot(kind, g, me),
            send_sem=deal_send.at[kind, g, d],
            recv_sem=deal_recv.at[kind, g, d],
            device_id={"sp": team * TEAM + peer},
            device_id_type=MESH,
        )

    def source(d):
        return lax.rem(me + TEAM - d, TEAM)

    def wait_deal(kind, g, d):
        here = slot(kind, g, source(d))
        pltpu.make_async_remote_copy(
            src_ref=here, dst_ref=here,
            send_sem=deal_send.at[kind, g, d], recv_sem=deal_recv.at[kind, g, d],
            device_id={"sp": team * TEAM + source(d)}, device_id_type=MESH,
        ).wait_recv()

    def hop(kind, index, src, dst):
        return pltpu.make_async_remote_copy(
            src_ref=src, dst_ref=dst,
            send_sem=hop_send.at[kind - 1, index], recv_sem=hop_recv.at[kind - 1, index],
            device_id={"sp": lax.rem(sp + TEAM, n_sp)}, device_id_type=MESH,
        )

    def first_hop(kind, s):
        return hop(kind, s, kv2.at[kind - 1, 2 * TEAM + s], kv2.at[kind - 1, TEAM + s])

    def second_hop(kind, s):
        return hop(kind, TEAM + s, kv2.at[kind - 1, TEAM + s], kv2.at[kind - 1, s])

    def near_hop(kind, i):
        return hop(kind, 2 * TEAM + i, kv1.at[kind - 1, TEAM + i], kv1.at[kind - 1, i])

    def edge_hop(kind):
        return hop(
            kind, 2 * TEAM + 2,
            kv0.at[kind - 1, pl.ds(span, KEYS)], kv0.at[kind - 1, pl.ds(0, KEYS)],
        )

    def forward(kind, g, s):
        if g == 2:
            pl.when(has_next)(lambda: first_hop(kind, s).start())
        elif g == 1:
            pl.when(has_next & (s >= TEAM - 2))(lambda: near_hop(kind, s - (TEAM - 2)).start())
        else:
            pl.when(has_next & (s == TEAM - 1))(lambda: edge_hop(kind).start())

    def relay(d):
        s = source(d)
        for kind in (V, K):

            @pl.when(has_prev)
            def _():
                first_hop(kind, s).wait_recv()

            @pl.when(has_prev & has_next)
            def _():
                second_hop(kind, s).start()

    def place(kind, g):
        slot(kind, g, me)[...] = ready[kind, g, :, lanes_of(me)]

    def arrive(g, d):
        for kind in (V, K):
            wait_deal(kind, g, d)
            forward(kind, g, source(d))

    barrier_waited = False
    for n, (kind, g) in enumerate(order):
        prepare(kind, g)
        place(kind, g)
        if not barrier_waited:
            count = TEAM + has_next.astype(jnp.int32) + has_prev.astype(jnp.int32)
            pl.semaphore_wait(barrier, count)
            barrier_waited = True
        for d in range(1, TEAM):
            deal(kind, g, d).start()
        if kind != Q:
            forward(kind, g, me)
        if n == 3:
            arrive(2, 1)
        if n == 5:
            arrive(2, 2)
    arrive(2, 3)
    relay(0)
    relay(1)
    for d in range(1, TEAM):
        arrive(1, d)
    relay(2)
    relay(3)
    for d in range(1, TEAM):
        arrive(0, d)

    @pl.when(jnp.logical_not(has_prev))
    def _():
        for kind in range(2):
            kv0[kind, 0:KEYS, :] = jnp.zeros((KEYS, part), BF16)
            for s in range(2):
                kv1[kind, s] = jnp.zeros((tokens, part), BF16)
            for s in range(TEAM):
                kv2[kind, TEAM + s] = jnp.zeros((tokens, part), BF16)

    @pl.when(jnp.logical_not(has_prev2))
    def _():
        for kind in range(2):
            for s in range(TEAM):
                kv2[kind, s] = jnp.zeros((tokens, part), BF16)

    def attend(g, head, query, key, value, index, start):
        rows, seen = query.shape[0], key.shape[0]
        a = lax.broadcasted_iota(jnp.int32, (rows, seen), 0)
        b = lax.broadcasted_iota(jnp.int32, (rows, seen), 1)
        allowed = (b >= jnp.maximum(a, KEYS - index)) & (b <= a + KEYS)
        scores = lax.dot_general(
            query, key, (((1,), (1,)), ((), ())), preferred_element_type=F32
        )
        scores = jnp.where(allowed, scores, MASKED)
        best = jnp.max(scores, axis=1, keepdims=True)
        weights = jnp.exp(scores - best)
        total = jnp.sum(weights, axis=1, keepdims=True)
        out = jnp.dot(weights.astype(BF16), value, preferred_element_type=F32)
        where = pl.ds(start, rows, stride=STRIDES[g]) if g else pl.ds(start, rows)
        acc[g, head, where, :] = out
        top[g, head, where, :] = jnp.broadcast_to(best, (rows, HEAD))
        den[g, head, where, :] = jnp.broadcast_to(total, (rows, HEAD))

    def cols(head):
        return slice(head * HEAD, (head + 1) * HEAD)

    for d in range(1, TEAM):
        wait_deal(Q, 1, d)

    @pl.when(has_prev)
    def _():
        for kind in (V, K):
            for i in range(2):
                near_hop(kind, i).wait_recv()

    each = tokens // STRIDES[1]
    pair = KEYS // each

    def step1(n, carry):
        r, i = n // (TEAM // pair), lax.rem(n, TEAM // pair)
        rows = pl.ds(pl.multiple_of(r * each, each), each)
        for head in range(mine):
            query = q_buf[1, pl.ds(i * pair, pair), rows, cols(head)].reshape(KEYS, HEAD)
            key = kv1[0, pl.ds(i * pair, 2 * pair), rows, cols(head)].reshape(2 * KEYS, HEAD)
            value = kv1[1, pl.ds(i * pair, 2 * pair), rows, cols(head)].reshape(2 * KEYS, HEAD)
            attend(1, head, query, key, value,
                   team * (span // STRIDES[1]) + i * KEYS, r + STRIDES[1] * KEYS * i)
        return carry

    lax.fori_loop(0, STRIDES[1] * (TEAM // pair), step1, 0, unroll=2)

    for d in range(1, TEAM):
        wait_deal(Q, 0, d)

    @pl.when(has_prev)
    def _():
        for kind in (V, K):
            edge_hop(kind).wait_recv()

    per = tokens // KEYS

    def step0(n, carry):
        inner = pl.ds(pl.multiple_of(lax.rem(n, per) * KEYS, KEYS), KEYS)
        rows = pl.ds(pl.multiple_of(n * KEYS, KEYS), 2 * KEYS)
        for head in range(mine):
            query = q_buf[0, n // per, inner, cols(head)]
            attend(0, head, query, kv0[0, rows, cols(head)], kv0[1, rows, cols(head)],
                   team * span + n * KEYS, pl.multiple_of(n * KEYS, KEYS))
        return carry

    lax.fori_loop(0, span // KEYS, step0, 0, unroll=2)

    for d in range(1, TEAM):
        wait_deal(Q, 2, d)

    @pl.when(has_prev2)
    def _():
        for d in range(TEAM):
            for kind in (V, K):
                second_hop(kind, source(d)).wait_recv()

    few = tokens // STRIDES[2]

    def step2(r, carry):
        rows = pl.ds(pl.multiple_of(r * few, few), few)
        for head in range(mine):
            query = q_buf[2, :, rows, cols(head)].reshape(TEAM * few, HEAD)
            key = kv2[0, :, rows, cols(head)].reshape(3 * TEAM * few, HEAD)
            value = kv2[1, :, rows, cols(head)].reshape(3 * TEAM * few, HEAD)
            attend(2, head, query, key, value, team * (span // STRIDES[2]), r)
        return carry

    lax.fori_loop(0, STRIDES[2], step2, 0, unroll=2)

    def merge(j):
        rows = pl.ds(pl.multiple_of(j * tokens, tokens), tokens)
        for head in range(mine):
            peak = jnp.maximum(
                jnp.maximum(top[0, head, rows, :], top[1, head, rows, :]), top[2, head, rows, :]
            )
            upper = jnp.zeros((tokens, HEAD), F32)
            lower = jnp.zeros((tokens, HEAD), F32)
            for g in range(3):
                scale = jnp.exp(top[g, head, rows, :] - peak)
                upper = upper + scale * acc[g, head, rows, :]
                lower = lower + scale * den[g, head, rows, :]
            att[j, :, cols(head)] = (upper / lower).astype(BF16)

    def home(d):
        peer = lax.rem(me + d, TEAM)
        return pltpu.make_async_remote_copy(
            src_ref=att.at[peer], dst_ref=full.at[tp, me],
            send_sem=ret_send.at[d], recv_sem=ret_recv.at[d],
            device_id={"sp": team * TEAM + peer}, device_id_type=MESH,
        )

    def twin(d, half):
        here = full.at[half, source(d)]
        return pltpu.make_async_remote_copy(
            src_ref=here, dst_ref=here,
            send_sem=d2d_send.at[d], recv_sem=d2d_recv.at[d],
            device_id={"tp": 1 - tp}, device_id_type=MESH,
        )

    for d in (2, 1, 3, 0):
        merge(lax.rem(me + d, TEAM))
        if d:
            home(d).start()
    full[tp, me] = att[me]
    twin(0, tp).start()
    w_copy.wait()

    def project(half, s):
        start = pl.multiple_of(half * width + s * part, part)
        return jnp.dot(full[half, s], w_buf[pl.ds(start, part), :], preferred_element_type=F32)

    result = acc_view = None
    total = project(tp, me)
    for d in (1, 3, 2):
        here = full.at[tp, source(d)]
        pltpu.make_async_remote_copy(
            src_ref=here, dst_ref=here, send_sem=ret_send.at[d], recv_sem=ret_recv.at[d],
            device_id={"sp": team * TEAM + source(d)}, device_id_type=MESH,
        ).wait_recv()
        twin(d, tp).start()
        total = total + project(tp, source(d))
    for d in (0, 1, 3, 2):
        twin(d, 1 - tp).wait_recv()
        total = total + project(1 - tp, source(d))
    o_ref[...] = total.astype(BF16)

    for kind, g in order:
        for d in range(1, TEAM):
            deal(kind, g, d).wait_send()
    for d in range(1, TEAM):
        home(d).wait_send()
    for d in range(TEAM):
        twin(d, tp).wait_send()

    @pl.when(has_next)
    def _():
        for kind in (V, K):
            for s in range(TEAM):
                first_hop(kind, s).wait_send()
            for i in range(2):
                near_hop(kind, i).wait_send()
            edge_hop(kind).wait_send()

    @pl.when(has_prev & has_next)
    def _():
        for kind in (V, K):
            for s in range(TEAM):
                second_hop(kind, s).wait_send()


def shards(n_sp, queries, keys, values, w_out):
    tokens, width = queries.shape[1:]
    heads = width // HEAD
    mine = heads // TEAM
    part = mine * HEAD
    span = TEAM * tokens
    start = lax.axis_index("sp") * tokens
    positions = (lax.iota(jnp.int32, tokens) + start).astype(F32)
    inverse = ROPE_BASE ** (-jnp.arange(0, HEAD, 2, dtype=F32) / HEAD)
    angles = positions[:, None] * inverse[None, :]
    cosine, sine = jnp.cos(angles), jnp.sin(angles)
    cosine = jnp.concatenate([cosine, cosine], axis=1)
    sine = jnp.concatenate([-sine, sine], axis=1)
    any_spec = pl.BlockSpec(memory_space=pl.ANY)
    vmem = pl.BlockSpec(memory_space=pltpu.VMEM)
    dma = pltpu.SemaphoreType.DMA
    return pl.pallas_call(
        functools.partial(kernel, (tokens, n_sp, heads)),
        out_shape=jax.ShapeDtypeStruct((tokens, w_out.shape[1]), BF16),
        in_specs=[any_spec] * 4 + [vmem] * 2,
        out_specs=vmem,
        scratch_shapes=[
            pltpu.VMEM((3, 3, tokens, width), BF16),
            pltpu.VMEM((3, 3, tokens, width), BF16),
            pltpu.VMEM(w_out.shape, BF16),
            pltpu.VMEM((2, 3, tokens, HEAD), F32),
            pltpu.VMEM((2, tokens, tokens), BF16),
            pltpu.VMEM((3, TEAM, tokens, part), BF16),
            pltpu.VMEM((2, KEYS + span, part), BF16),
            pltpu.VMEM((2, 2 + TEAM, tokens, part), BF16),
            pltpu.VMEM((2, 3 * TEAM, tokens, part), BF16),
            pltpu.VMEM((3, mine, span, HEAD), F32),
            pltpu.VMEM((3, mine, span, HEAD), F32),
            pltpu.VMEM((3, mine, span, HEAD), F32),
            pltpu.VMEM((TEAM, tokens, part), BF16),
            pltpu.VMEM((2, TEAM, tokens, part), BF16),
            dma((3, 3)),
            dma,
            dma((3, 3, TEAM)),
            dma((3, 3, TEAM)),
            dma((2, 2 * TEAM + 3)),
            dma((2, 2 * TEAM + 3)),
            dma((TEAM,)),
            dma((TEAM,)),
            dma((TEAM,)),
            dma((TEAM,)),
        ],
        compiler_params=pltpu.CompilerParams(
            collective_id=0, has_side_effects=True, vmem_limit_bytes=60 * 1024 * 1024
        ),
    )(queries, keys, values, w_out, cosine, sine)


def solution(mesh):
    return jax.shard_map(
        functools.partial(shards, mesh.shape["sp"]),
        mesh=mesh,
        in_specs=(P(None, "sp", "tp"), P(None, "sp", "tp"), P(None, "sp", "tp"), P(None, "tp")),
        out_specs=P("sp", "tp"),
        check_vma=False,
    )
```

time: 432 us -> 90.8 us (0.21)
  waiting for transfers between devices: 242 us -> 0 us
  local copies, waits for them, and re-layouts: 114 us -> 1.87 us
  Pallas kernels: 0 us -> 85.9 us
  other arithmetic: 25.3 us -> 1.39 us
  matrix products: 21.3 us -> 0 us
  starting transfers between devices: 14 us -> 0 us
  between operations: 14 us -> 0.02 us
    ppermute x5 -> x0, waiting for transfers between devices: 195 us -> none  [shifted(): return lax.ppermute(block, axis, route)]
    pallas_call x0 -> x1, Pallas kernels: none -> 85.9 us  [shards(): pl.pallas_call(functools.partial(kernel, (tokens, n_sp, heads)), out_shap...]
    unnamed x80 -> x1, local copies, waits for them, and re-layouts: 54.5 us -> 1.87 us
    all_gather x1 -> x0, waiting for transfers between devices: 46.3 us -> none  [shards(): lax.all_gather(attended, 'tp', axis=1, tiled=True)]
    slice x13 -> x0, local copies, waits for them, and re-layouts: 37.1 us -> none  [the longest x4 19.2 us: local_window(): extended[0].reshape(strided + KEYS_PER_QUERY, dilation, head_count, HEAD)]
    dot_general x7 -> x0, matrix products: 21.3 us -> none  [the longest x3 9.41 us: local_window(): jnp.einsum('nqrhe,nkrhe->nrhqk', q_blocks, key_blocks, preferred_element_...]
    ppermute x5 -> x0, starting transfers between devices: 14 us -> none  [shifted(): return lax.ppermute(block, axis, route)]
    concatenate x7 -> x0, local copies, waits for them, and re-layouts: 8.17 us -> none  [turn_halves(): jnp.concatenate([first_half * cosine - second_half * sine_part, second_ha...]
  transfers between devices with their start and end apart: 6 -> 0, of which waited for: 5 -> 0; matrix products, arithmetic and copies ran while one was open for 6% -> 0% of each run, Pallas kernels for 0% -> 0%
where the time goes in v1:
time: 90.8 us; the launch traced here: 89.2 us
  Pallas kernels  85.9 us (95%)
  local copies, waits for them, and re-layouts  1.87 us (2%)
  other arithmetic  1.39 us (2%)
    pallas_call x1, Pallas kernels, shards(): pl.pallas_call(functools.partial(kernel, (tokens, n_sp, heads)), out_shap...  85.9 us
    unnamed x1, local copies, waits for them, and re-layouts  1.87 us

profile of v1, /device:TPU:21, one launch (start us, length us, event | category | flops | bytes accessed | tf_op | source)
XLA Modules:
  0.0 89.2 jit_solution(8231695596058503041)
XLA Ops:
  0.0 0.5 fusion
  0.6 0.8 pad_maximum_fusion
  1.4 85.9 %shard_map.46 = bf16[256,1024]{1,0:T(8,128)(2,1)} custom-call(bf16[3,256,1024]{2,1,0:T(8,128)(2,1)} %q_in.1, bf16[3,256,1024]{2,1,0:T(8,128)(2,1)} %k_in.1, bf16[3,256,1024]{2,1,0:T(8,128)(2,1)} %v_in.1, bf16[2048,1024]{1,0:T(8,128)(2,1)} %w_in.1, f32[256,128]{1,0:T(8,128)} %get-tuple-element.8.cos_ref, f32[256,128]{1,0:T(8,128)} %get-tuple-element.9.sin_ref), custom_call_target="tpu_custom_call" | custom-call | tf_op jit(solution)/shard_map/pallas_call | solution.py:411
  87.3 1.9 %copy.6 = bf16[256,1024]{1,0:T(8,128)(2,1)} copy(bf16[256,1024]{1,0:T(8,128)(2,1)} %shard_map.46) | data formatting | bytes 1048576
  (2 shorter events, 0.0 us)

commit v2 on v1

--- a/solution.py
+++ b/solution.py
@@ -23,7 +23,7 @@
     cfg,
     q_in, k_in, v_in, w_in, cos_ref, sin_ref,
     o_ref,
-    raw, ready, w_buf, tables, perms, q_buf, kv0, kv1, kv2, acc, top, den, att, full,
+    raw, ready, w_buf, tables, perms, q_buf, kv0, kv1, kv2, acc, lse, bias, att, full, total_buf,
     in_sem, w_sem, deal_send, deal_recv, hop_send, hop_recv, ret_send, ret_recv, d2d_send, d2d_recv,
 ):
     tokens, n_sp, heads = cfg
@@ -47,8 +47,18 @@
         copy = pltpu.make_async_copy(inputs[kind].at[g], raw.at[kind, g], in_sem.at[kind, g])
         copy.start()
         loads[kind, g] = copy
-    w_copy = pltpu.make_async_copy(w_in, w_buf, w_sem)
-    w_copy.start()
+    w_loads = []
+    for half in range(2):
+        for head in range(mine):
+            for s in range(TEAM):
+                rows = pl.ds(half * width + s * part + head * HEAD, HEAD)
+                copy = pltpu.make_async_copy(
+                    w_in.at[rows],
+                    w_buf.at[half, head, pl.ds(s * HEAD, HEAD)],
+                    w_sem.at[half, head, s],
+                )
+                copy.start()
+                w_loads.append(copy)
 
     barrier = pltpu.get_barrier_semaphore()
     for d in range(1, TEAM):
@@ -106,6 +116,9 @@
             return kv1.at[kind - 1, 2 + s]
         return kv0.at[kind - 1, pl.ds(pl.multiple_of(KEYS + s * tokens, KEYS), tokens)]
 
+    def cols(head):
+        return slice(head * HEAD, (head + 1) * HEAD)
+
     def lanes_of(j):
         return pl.ds(pl.multiple_of(j * part, part), part)
 
@@ -131,6 +144,8 @@
             device_id={"sp": team * TEAM + source(d)}, device_id_type=MESH,
         ).wait_recv()
 
+    near = TEAM * (1 + mine)
+
     def hop(kind, index, src, dst):
         return pltpu.make_async_remote_copy(
             src_ref=src, dst_ref=dst,
@@ -141,15 +156,18 @@
     def first_hop(kind, s):
         return hop(kind, s, kv2.at[kind - 1, 2 * TEAM + s], kv2.at[kind - 1, TEAM + s])
 
-    def second_hop(kind, s):
-        return hop(kind, TEAM + s, kv2.at[kind - 1, TEAM + s], kv2.at[kind - 1, s])
+    def second_hop(kind, s, head):
+        return hop(
+            kind, TEAM * (1 + head) + s,
+            kv2.at[kind - 1, TEAM + s, :, cols(head)], kv2.at[kind - 1, s, :, cols(head)],
+        )
 
     def near_hop(kind, i):
-        return hop(kind, 2 * TEAM + i, kv1.at[kind - 1, TEAM + i], kv1.at[kind - 1, i])
+        return hop(kind, near + i, kv1.at[kind - 1, TEAM + i], kv1.at[kind - 1, i])
 
     def edge_hop(kind):
         return hop(
-            kind, 2 * TEAM + 2,
+            kind, near + 2,
             kv0.at[kind - 1, pl.ds(span, KEYS)], kv0.at[kind - 1, pl.ds(0, KEYS)],
         )
 
@@ -161,17 +179,18 @@
         else:
             pl.when(has_next & (s == TEAM - 1))(lambda: edge_hop(kind).start())
 
-    def relay(d):
+    def relay(d, head):
         s = source(d)
         for kind in (V, K):
-
-            @pl.when(has_prev)
-            def _():
-                first_hop(kind, s).wait_recv()
+            if head == 0:
+
+                @pl.when(has_prev)
+                def _():
+                    first_hop(kind, s).wait_recv()
 
             @pl.when(has_prev & has_next)
             def _():
-                second_hop(kind, s).start()
+                second_hop(kind, s, head).start()
 
     def place(kind, g):
         slot(kind, g, me)[...] = ready[kind, g, :, lanes_of(me)]
@@ -198,14 +217,17 @@
         if n == 5:
             arrive(2, 2)
     arrive(2, 3)
-    relay(0)
-    relay(1)
+    relay(0, 0)
+    relay(1, 0)
     for d in range(1, TEAM):
         arrive(1, d)
-    relay(2)
-    relay(3)
+    relay(2, 0)
+    relay(3, 0)
     for d in range(1, TEAM):
         arrive(0, d)
+    for head in range(1, mine):
+        for d in range(TEAM):
+            relay(d, head)
 
     @pl.when(jnp.logical_not(has_prev))
     def _():
@@ -222,26 +244,30 @@
             for s in range(TEAM):
                 kv2[kind, s] = jnp.zeros((tokens, part), BF16)
 
-    def attend(g, head, query, key, value, index, start):
-        rows, seen = query.shape[0], key.shape[0]
-        a = lax.broadcasted_iota(jnp.int32, (rows, seen), 0)
-        b = lax.broadcasted_iota(jnp.int32, (rows, seen), 1)
+    few = tokens // STRIDES[2]
+
+    def fill(index, rows):
+        a = lax.broadcasted_iota(jnp.int32, (rows, rows + KEYS), 0)
+        b = lax.broadcasted_iota(jnp.int32, (rows, rows + KEYS), 1)
         allowed = (b >= jnp.maximum(a, KEYS - index)) & (b <= a + KEYS)
+        return jnp.where(allowed, 0.0, MASKED)
+
+    bias[0] = fill(team * span, KEYS)
+    bias[1] = fill(KEYS, KEYS)
+    bias[2, 0 : TEAM * few, 0 : TEAM * few + KEYS] = fill(team * TEAM * few, TEAM * few)
+
+    def attend(g, head, query, key, value, off, start):
+        rows = query.shape[0]
         scores = lax.dot_general(
             query, key, (((1,), (1,)), ((), ())), preferred_element_type=F32
-        )
-        scores = jnp.where(allowed, scores, MASKED)
+        ) + off
         best = jnp.max(scores, axis=1, keepdims=True)
         weights = jnp.exp(scores - best)
         total = jnp.sum(weights, axis=1, keepdims=True)
-        out = jnp.dot(weights.astype(BF16), value, preferred_element_type=F32)
+        out = jnp.dot(weights.astype(BF16), value, preferred_element_type=F32) / total
         where = pl.ds(start, rows, stride=STRIDES[g]) if g else pl.ds(start, rows)
         acc[g, head, where, :] = out
-        top[g, head, where, :] = jnp.broadcast_to(best, (rows, HEAD))
-        den[g, head, where, :] = jnp.broadcast_to(total, (rows, HEAD))
-
-    def cols(head):
-        return slice(head * HEAD, (head + 1) * HEAD)
+        lse[g, head, where, :] = jnp.broadcast_to(best + jnp.log(total), (rows, HEAD))
 
     for d in range(1, TEAM):
         wait_deal(Q, 1, d)
@@ -263,7 +289,7 @@
             key = kv1[0, pl.ds(i * pair, 2 * pair), rows, cols(head)].reshape(2 * KEYS, HEAD)
             value = kv1[1, pl.ds(i * pair, 2 * pair), rows, cols(head)].reshape(2 * KEYS, HEAD)
             attend(1, head, query, key, value,
-                   team * (span // STRIDES[1]) + i * KEYS, r + STRIDES[1] * KEYS * i)
+                   bias[jnp.minimum(i, 1)], r + STRIDES[1] * KEYS * i)
         return carry
 
     lax.fori_loop(0, STRIDES[1] * (TEAM // pair), step1, 0, unroll=2)
@@ -284,7 +310,7 @@
         for head in range(mine):
             query = q_buf[0, n // per, inner, cols(head)]
             attend(0, head, query, kv0[0, rows, cols(head)], kv0[1, rows, cols(head)],
-                   team * span + n * KEYS, pl.multiple_of(n * KEYS, KEYS))
+                   bias[jnp.minimum(n, 1)], pl.multiple_of(n * KEYS, KEYS))
         return carry
 
     lax.fori_loop(0, span // KEYS, step0, 0, unroll=2)
@@ -292,89 +318,97 @@
     for d in range(1, TEAM):
         wait_deal(Q, 2, d)
 
-    @pl.when(has_prev2)
-    def _():
-        for d in range(TEAM):
-            for kind in (V, K):
-                second_hop(kind, source(d)).wait_recv()
-
-    few = tokens // STRIDES[2]
-
-    def step2(r, carry):
-        rows = pl.ds(pl.multiple_of(r * few, few), few)
-        for head in range(mine):
+    def far(head):
+        def step(r, carry):
+            rows = pl.ds(pl.multiple_of(r * few, few), few)
             query = q_buf[2, :, rows, cols(head)].reshape(TEAM * few, HEAD)
             key = kv2[0, :, rows, cols(head)].reshape(3 * TEAM * few, HEAD)
             value = kv2[1, :, rows, cols(head)].reshape(3 * TEAM * few, HEAD)
-            attend(2, head, query, key, value, team * (span // STRIDES[2]), r)
-        return carry
-
-    lax.fori_loop(0, STRIDES[2], step2, 0, unroll=2)
-
-    def merge(j):
+            attend(2, head, query, key, value, bias[2, 0 : TEAM * few, 0 : TEAM * few + KEYS], r)
+            return carry
+
+        lax.fori_loop(0, STRIDES[2], step, 0, unroll=4)
+
+    def merge(j, head):
         rows = pl.ds(pl.multiple_of(j * tokens, tokens), tokens)
-        for head in range(mine):
-            peak = jnp.maximum(
-                jnp.maximum(top[0, head, rows, :], top[1, head, rows, :]), top[2, head, rows, :]
-            )
-            upper = jnp.zeros((tokens, HEAD), F32)
-            lower = jnp.zeros((tokens, HEAD), F32)
-            for g in range(3):
-                scale = jnp.exp(top[g, head, rows, :] - peak)
-                upper = upper + scale * acc[g, head, rows, :]
-                lower = lower + scale * den[g, head, rows, :]
-            att[j, :, cols(head)] = (upper / lower).astype(BF16)
-
-    def home(d):
+        logs = [lse[g, head, rows, :] for g in range(3)]
+        peak = jnp.maximum(jnp.maximum(logs[0], logs[1]), logs[2])
+        upper = jnp.zeros((tokens, HEAD), F32)
+        lower = jnp.zeros((tokens, HEAD), F32)
+        for g in range(3):
+            scale = jnp.exp(logs[g] - peak)
+            upper = upper + scale * acc[g, head, rows, :]
+            lower = lower + scale
+        att[head, j] = (upper / lower).astype(BF16)
+
+    def place_of(s):
+        return pl.ds(pl.multiple_of(s * HEAD, HEAD), HEAD)
+
+    def home(d, head):
         peer = lax.rem(me + d, TEAM)
         return pltpu.make_async_remote_copy(
-            src_ref=att.at[peer], dst_ref=full.at[tp, me],
-            send_sem=ret_send.at[d], recv_sem=ret_recv.at[d],
+            src_ref=att.at[head, peer], dst_ref=full.at[tp, head, :, place_of(me)],
+            send_sem=ret_send.at[d, head], recv_sem=ret_recv.at[d, head],
             device_id={"sp": team * TEAM + peer}, device_id_type=MESH,
         )
 
-    def twin(d, half):
-        here = full.at[half, source(d)]
+    def wait_home(d, head):
+        here = full.at[tp, head, :, place_of(source(d))]
+        pltpu.make_async_remote_copy(
+            src_ref=here, dst_ref=here,
+            send_sem=ret_send.at[d, head], recv_sem=ret_recv.at[d, head],
+            device_id={"sp": team * TEAM + source(d)}, device_id_type=MESH,
+        ).wait_recv()
+
+    def twin(d, half, head):
+        here = full.at[half, head, :, place_of(source(d))]
         return pltpu.make_async_remote_copy(
             src_ref=here, dst_ref=here,
-            send_sem=d2d_send.at[d], recv_sem=d2d_recv.at[d],
+            send_sem=d2d_send.at[d, head], recv_sem=d2d_recv.at[d, head],
             device_id={"tp": 1 - tp}, device_id_type=MESH,
         )
 
-    for d in (2, 1, 3, 0):
-        merge(lax.rem(me + d, TEAM))
-        if d:
-            home(d).start()
-    full[tp, me] = att[me]
-    twin(0, tp).start()
-    w_copy.wait()
-
-    def project(half, s):
-        start = pl.multiple_of(half * width + s * part, part)
-        return jnp.dot(full[half, s], w_buf[pl.ds(start, part), :], preferred_element_type=F32)
-
-    result = acc_view = None
-    total = project(tp, me)
-    for d in (1, 3, 2):
-        here = full.at[tp, source(d)]
-        pltpu.make_async_remote_copy(
-            src_ref=here, dst_ref=here, send_sem=ret_send.at[d], recv_sem=ret_recv.at[d],
-            device_id={"sp": team * TEAM + source(d)}, device_id_type=MESH,
-        ).wait_recv()
-        twin(d, tp).start()
-        total = total + project(tp, source(d))
-    for d in (0, 1, 3, 2):
-        twin(d, 1 - tp).wait_recv()
-        total = total + project(1 - tp, source(d))
-    o_ref[...] = total.astype(BF16)
+    for copy in w_loads:
+        copy.wait()
+    for head in range(mine):
+
+        @pl.when(has_prev2)
+        def _():
+            for d in range(TEAM):
+                for kind in (V, K):
+                    second_hop(kind, source(d), head).wait_recv()
+
+        far(head)
+        for d in (2, 1, 3, 0):
+            merge(lax.rem(me + d, TEAM), head)
+            if d:
+                home(d, head).start()
+        full[tp, head, :, place_of(me)] = att[head, me]
+        twin(0, tp, head).start()
+        for d in (1, 3, 2):
+            wait_home(d, head)
+            twin(d, tp, head).start()
+        product = jnp.dot(full[tp, head], w_buf[tp, head], preferred_element_type=F32)
+        for d in range(TEAM):
+            twin(d, 1 - tp, head).wait_recv()
+        product = product + jnp.dot(
+            full[1 - tp, head], w_buf[1 - tp, head], preferred_element_type=F32
+        )
+        if head == 0:
+            total_buf[...] = product
+        elif head < mine - 1:
+            total_buf[...] += product
+        else:
+            o_ref[...] = (total_buf[...] + product).astype(BF16)
 
     for kind, g in order:
         for d in range(1, TEAM):
             deal(kind, g, d).wait_send()
-    for d in range(1, TEAM):
-        home(d).wait_send()
-    for d in range(TEAM):
-        twin(d, tp).wait_send()
+    for head in range(mine):
+        for d in range(1, TEAM):
+            home(d, head).wait_send()
+        for d in range(TEAM):
+            twin(d, tp, head).wait_send()
 
     @pl.when(has_next)
     def _():
@@ -389,7 +423,8 @@
     def _():
         for kind in (V, K):
             for s in range(TEAM):
-                second_hop(kind, s).wait_send()
+                for head in range(mine):
+                    second_hop(kind, s, head).wait_send()
 
 
 def shards(n_sp, queries, keys, values, w_out):
@@ -416,7 +451,7 @@
         scratch_shapes=[
             pltpu.VMEM((3, 3, tokens, width), BF16),
             pltpu.VMEM((3, 3, tokens, width), BF16),
-            pltpu.VMEM(w_out.shape, BF16),
+            pltpu.VMEM((2, mine, TEAM * HEAD, w_out.shape[1]), BF16),
             pltpu.VMEM((2, 3, tokens, HEAD), F32),
             pltpu.VMEM((2, tokens, tokens), BF16),
             pltpu.VMEM((3, TEAM, tokens, part), BF16),
@@ -425,19 +460,20 @@
             pltpu.VMEM((2, 3 * TEAM, tokens, part), BF16),
             pltpu.VMEM((3, mine, span, HEAD), F32),
             pltpu.VMEM((3, mine, span, HEAD), F32),
-            pltpu.VMEM((3, mine, span, HEAD), F32),
-            pltpu.VMEM((TEAM, tokens, part), BF16),
-            pltpu.VMEM((2, TEAM, tokens, part), BF16),
+            pltpu.VMEM((3, KEYS, 2 * KEYS), F32),
+            pltpu.VMEM((mine, TEAM, tokens, HEAD), BF16),
+            pltpu.VMEM((2, mine, tokens, TEAM * HEAD), BF16),
+            pltpu.VMEM((tokens, w_out.shape[1]), F32),
             dma((3, 3)),
-            dma,
+            dma((2, mine, TEAM)),
             dma((3, 3, TEAM)),
             dma((3, 3, TEAM)),
-            dma((2, 2 * TEAM + 3)),
-            dma((2, 2 * TEAM + 3)),
-            dma((TEAM,)),
-            dma((TEAM,)),
-            dma((TEAM,)),
-            dma((TEAM,)),
+            dma((2, TEAM * (1 + mine) + 3)),
+            dma((2, TEAM * (1 + mine) + 3)),
+            dma((TEAM, mine)),
+            dma((TEAM, mine)),
+            dma((TEAM, mine)),
+            dma((TEAM, mine)),
         ],
         compiler_params=pltpu.CompilerParams(
             collective_id=0, has_side_effects=True, vmem_limit_bytes=60 * 1024 * 1024

time: 90.8 us -> 87.9 us (0.968); the launches traced: 89.2 us -> 87.7 us
  Pallas kernels: 85.9 us -> 84.4 us
    pallas_call x1, Pallas kernels: 85.9 us -> 84.4 us  [shards(): pl.pallas_call(functools.partial(kernel, (tokens, n_sp, heads)), out_shap...]
where the time goes in v2:
time: 87.9 us; the launch traced here: 87.7 us
  Pallas kernels  84.4 us (96%)
  local copies, waits for them, and re-layouts  1.87 us (2%)
  other arithmetic  1.39 us (2%)
    pallas_call x1, Pallas kernels, shards(): pl.pallas_call(functools.partial(kernel, (tokens, n_sp, heads)), out_shap...  84.4 us
    unnamed x1, local copies, waits for them, and re-layouts  1.87 us

profile of v2, /device:TPU:21, one launch (start us, length us, event | category | flops | bytes accessed | tf_op | source)
XLA Modules:
  0.0 87.7 jit_solution(2030707935428007684)
XLA Ops:
  0.0 0.5 fusion
  0.6 0.8 pad_maximum_fusion
  1.4 84.4 %shard_map.46 = bf16[256,1024]{1,0:T(8,128)(2,1)} custom-call(bf16[3,256,1024]{2,1,0:T(8,128)(2,1)} %q_in.1, bf16[3,256,1024]{2,1,0:T(8,128)(2,1)} %k_in.1, bf16[3,256,1024]{2,1,0:T(8,128)(2,1)} %v_in.1, bf16[2048,1024]{1,0:T(8,128)(2,1)} %w_in.1, f32[256,128]{1,0:T(8,128)} %get-tuple-element.8.cos_ref, f32[256,128]{1,0:T(8,128)} %get-tuple-element.9.sin_ref), custom_call_target="tpu_custom_call" | custom-call | tf_op jit(solution)/shard_map/pallas_call | solution.py:446
  85.8 1.9 %copy.6 = bf16[256,1024]{1,0:T(8,128)(2,1)} copy(bf16[256,1024]{1,0:T(8,128)(2,1)} %shard_map.46) | data formatting | bytes 1048576
  (2 shorter events, 0.0 us)

commit v3 on v2

--- a/solution.py
+++ b/solution.py
@@ -41,7 +41,7 @@
 
     inputs = (q_in, k_in, v_in)
     Q, K, V = 0, 1, 2
-    order = [(V, 2), (K, 2), (V, 1), (K, 1), (V, 0), (K, 0), (Q, 1), (Q, 0), (Q, 2)]
+    order = [(V, 2), (K, 2), (V, 1), (K, 1), (V, 0), (K, 0), (Q, 2), (Q, 1), (Q, 0)]
     loads = {}
     for kind, g in order:
         copy = pltpu.make_async_copy(inputs[kind].at[g], raw.at[kind, g], in_sem.at[kind, g])
@@ -76,12 +76,13 @@
 
     row = lax.broadcasted_iota(jnp.int32, (tokens, tokens), 0)
     col = lax.broadcasted_iota(jnp.int32, (tokens, tokens), 1)
-    for g in (1, 2):
-        stride = STRIDES[g]
-        each = tokens // stride
-        origin = lax.rem(row, each) * stride + row // each
+
+    def sorter(g):
+        each = tokens // STRIDES[g]
+        origin = lax.rem(row, each) * STRIDES[g] + row // each
         perms[g - 1] = jnp.where(origin == col, 1.0, 0.0).astype(BF16)
-    for g in range(3):
+
+    def sort_tables(g):
         stride = STRIDES[g]
         each = tokens // stride
         for r in range(stride):
@@ -202,6 +203,10 @@
 
     barrier_waited = False
     for n, (kind, g) in enumerate(order):
+        if kind == V and g > 0:
+            sorter(g)
+        if kind == K:
+            sort_tables(g)
         prepare(kind, g)
         place(kind, g)
         if not barrier_waited:
@@ -256,18 +261,46 @@
     bias[1] = fill(KEYS, KEYS)
     bias[2, 0 : TEAM * few, 0 : TEAM * few + KEYS] = fill(team * TEAM * few, TEAM * few)
 
-    def attend(g, head, query, key, value, off, start):
-        rows = query.shape[0]
-        scores = lax.dot_general(
-            query, key, (((1,), (1,)), ((), ())), preferred_element_type=F32
-        ) + off
-        best = jnp.max(scores, axis=1, keepdims=True)
-        weights = jnp.exp(scores - best)
-        total = jnp.sum(weights, axis=1, keepdims=True)
-        out = jnp.dot(weights.astype(BF16), value, preferred_element_type=F32) / total
-        where = pl.ds(start, rows, stride=STRIDES[g]) if g else pl.ds(start, rows)
-        acc[g, head, where, :] = out
-        lse[g, head, where, :] = jnp.broadcast_to(best + jnp.log(total), (rows, HEAD))
+    def attend(g, tiles):
+        scores = [
+            lax.dot_general(t[1], t[2], (((1,), (1,)), ((), ())), preferred_element_type=F32)
+            + t[4]
+            for t in tiles
+        ]
+        best = [jnp.max(x, axis=1, keepdims=True) for x in scores]
+        weights = [jnp.exp(x - m) for x, m in zip(scores, best)]
+        outs = [
+            jnp.dot(p.astype(BF16), t[3], preferred_element_type=F32)
+            for p, t in zip(weights, tiles)
+        ]
+        total = [jnp.sum(p, axis=1, keepdims=True) for p in weights]
+        for t, out, m, l in zip(tiles, outs, best, total):
+            rows = out.shape[0]
+            where = pl.ds(t[5], rows, stride=STRIDES[g]) if g else pl.ds(t[5], rows)
+            acc[g, t[0], where, :] = out / l
+            lse[g, t[0], where, :] = jnp.broadcast_to(m + jnp.log(l), (rows, HEAD))
+
+    def far(head):
+        @pl.when(has_prev2)
+        def _():
+            for d in range(TEAM):
+                for kind in (V, K):
+                    second_hop(kind, source(d), head).wait_recv()
+
+        off = bias[2, 0 : TEAM * few, 0 : TEAM * few + KEYS]
+        for first in range(0, STRIDES[2], 4):
+            tiles = []
+            for r in range(first, first + 4):
+                rows = slice(r * few, (r + 1) * few)
+                query = q_buf[2, :, rows, cols(head)].reshape(TEAM * few, HEAD)
+                key = kv2[0, :, rows, cols(head)].reshape(3 * TEAM * few, HEAD)
+                value = kv2[1, :, rows, cols(head)].reshape(3 * TEAM * few, HEAD)
+                tiles.append((head, query, key, value, off, r))
+            attend(2, tiles)
+
+    for d in range(1, TEAM):
+        wait_deal(Q, 2, d)
+    far(0)
 
     for d in range(1, TEAM):
         wait_deal(Q, 1, d)
@@ -284,12 +317,14 @@
     def step1(n, carry):
         r, i = n // (TEAM // pair), lax.rem(n, TEAM // pair)
         rows = pl.ds(pl.multiple_of(r * each, each), each)
+        tiles = []
         for head in range(mine):
             query = q_buf[1, pl.ds(i * pair, pair), rows, cols(head)].reshape(KEYS, HEAD)
             key = kv1[0, pl.ds(i * pair, 2 * pair), rows, cols(head)].reshape(2 * KEYS, HEAD)
             value = kv1[1, pl.ds(i * pair, 2 * pair), rows, cols(head)].reshape(2 * KEYS, HEAD)
-            attend(1, head, query, key, value,
-                   bias[jnp.minimum(i, 1)], r + STRIDES[1] * KEYS * i)
+            tiles.append((head, query, key, value,
+                          bias[jnp.minimum(i, 1)], r + STRIDES[1] * KEYS * i))
+        attend(1, tiles)
         return carry
 
     lax.fori_loop(0, STRIDES[1] * (TEAM // pair), step1, 0, unroll=2)
@@ -307,27 +342,15 @@
     def step0(n, carry):
         inner = pl.ds(pl.multiple_of(lax.rem(n, per) * KEYS, KEYS), KEYS)
         rows = pl.ds(pl.multiple_of(n * KEYS, KEYS), 2 * KEYS)
+        tiles = []
         for head in range(mine):
             query = q_buf[0, n // per, inner, cols(head)]
-            attend(0, head, query, kv0[0, rows, cols(head)], kv0[1, rows, cols(head)],
-                   bias[jnp.minimum(n, 1)], pl.multiple_of(n * KEYS, KEYS))
+            tiles.append((head, query, kv0[0, rows, cols(head)], kv0[1, rows, cols(head)],
+                          bias[jnp.minimum(n, 1)], pl.multiple_of(n * KEYS, KEYS)))
+        attend(0, tiles)
         return carry
 
     lax.fori_loop(0, span // KEYS, step0, 0, unroll=2)
-
-    for d in range(1, TEAM):
-        wait_deal(Q, 2, d)
-
-    def far(head):
-        def step(r, carry):
-            rows = pl.ds(pl.multiple_of(r * few, few), few)
-            query = q_buf[2, :, rows, cols(head)].reshape(TEAM * few, HEAD)
-            key = kv2[0, :, rows, cols(head)].reshape(3 * TEAM * few, HEAD)
-            value = kv2[1, :, rows, cols(head)].reshape(3 * TEAM * few, HEAD)
-            attend(2, head, query, key, value, bias[2, 0 : TEAM * few, 0 : TEAM * few + KEYS], r)
-            return carry
-
-        lax.fori_loop(0, STRIDES[2], step, 0, unroll=4)
 
     def merge(j, head):
         rows = pl.ds(pl.multiple_of(j * tokens, tokens), tokens)
@@ -371,20 +394,15 @@
     for copy in w_loads:
         copy.wait()
     for head in range(mine):
-
-        @pl.when(has_prev2)
-        def _():
-            for d in range(TEAM):
-                for kind in (V, K):
-                    second_hop(kind, source(d), head).wait_recv()
-
-        far(head)
+        if head:
+            far(head)
         for d in (2, 1, 3, 0):
             merge(lax.rem(me + d, TEAM), head)
             if d:
                 home(d, head).start()
         full[tp, head, :, place_of(me)] = att[head, me]
         twin(0, tp, head).start()
+    for head in range(mine):
         for d in (1, 3, 2):
             wait_home(d, head)
             twin(d, tp, head).start()

time: 87.9 us -> 80.1 us (0.911)
  Pallas kernels: 84.4 us -> 75.8 us
    pallas_call x1, Pallas kernels: 84.4 us -> 75.8 us  [shards(): pl.pallas_call(functools.partial(kernel, (tokens, n_sp, heads)), out_shap...]
where the time goes in v3:
time: 80.1 us; the launch traced here: 79.1 us
  Pallas kernels  75.8 us (95%)
  local copies, waits for them, and re-layouts  1.87 us (2%)
  other arithmetic  1.39 us (2%)
    pallas_call x1, Pallas kernels, shards(): pl.pallas_call(functools.partial(kernel, (tokens, n_sp, heads)), out_shap...  75.8 us
    unnamed x1, local copies, waits for them, and re-layouts  1.87 us

profile of v3, /device:TPU:21, one launch (start us, length us, event | category | flops | bytes accessed | tf_op | source)
XLA Modules:
  0.0 79.1 jit_solution(17921909122780633788)
XLA Ops:
  0.0 0.5 fusion
  0.6 0.8 %pad_maximum_fusion = (f32[256,128]{1,0:T(8,128)}, f32[256,128]{1,0:T(8,128)}) fusion(f32[256,64]{1,0:T(8,128)S(1)} %get-tuple-element.7, f32[256,64]{1,0:T(8,128)S(1)} %get-tuple-element.6, f32[256,64]{1,0:T(8,128)S(1)} %get-tuple-element.5), kind=kLoop, calls=%fused_computation.2 | loop fusion | flops 65536 | bytes 458752 | tf_op jit(solution)/shard_map/concatenate | solution.py:459
  1.4 75.8 %shard_map.46 = bf16[256,1024]{1,0:T(8,128)(2,1)} custom-call(bf16[3,256,1024]{2,1,0:T(8,128)(2,1)} %q_in.1, bf16[3,256,1024]{2,1,0:T(8,128)(2,1)} %k_in.1, bf16[3,256,1024]{2,1,0:T(8,128)(2,1)} %v_in.1, bf16[2048,1024]{1,0:T(8,128)(2,1)} %w_in.1, f32[256,128]{1,0:T(8,128)} %get-tuple-element.8.cos_ref, f32[256,128]{1,0:T(8,128)} %get-tuple-element.9.sin_ref), custom_call_target="tpu_custom_call" | custom-call | tf_op jit(solution)/shard_map/pallas_call | solution.py:464
  77.2 1.9 %copy.6 = bf16[256,1024]{1,0:T(8,128)(2,1)} copy(bf16[256,1024]{1,0:T(8,128)(2,1)} %shard_map.46) | data formatting | bytes 1048576
  (2 shorter events, 0.0 us)
